TPU v7x, 512 devices: a whole 4x4x16 slice. The times are simulated.
512 devices in a mesh: sp: 64 (over z, y), tp: 8 (over x, core).
Axes of the slice: x: 4, y: 4, z: 16, core: 2. Of those that a mesh axis runs over, the one named last changes fastest.
Arguments:
- queries: bfloat16 [12288, 1024], P('sp', 'tp'), may hold values from -6 to 6
- keys: bfloat16 [12288, 512], P('sp', 'tp'), may hold values from -6 to 6
- values: bfloat16 [12288, 512], P('sp', 'tp'), may hold values from -6 to 6
- q_gain: float32 [64], replicated, may hold values from 0.1 to 6.5
- k_gain: float32 [64], replicated, may hold values from 0.1 to 6.5
- w_out: bfloat16 [1024, 2048], P('tp'), may hold values from -12 to 12
- residual: bfloat16 [12288, 2048], P(('sp', 'tp')), may hold values from -6 to 6
- norm_gain: float32 [2048], replicated, may hold values from 0.1 to 1.9
- w_gate: bfloat16 [2048, 5632], P('sp', 'tp'), may hold values from -0.125 to 0.125
- w_up: bfloat16 [2048, 5632], P('sp', 'tp'), may hold values from -0.125 to 0.125
- w_down: bfloat16 [5632, 2048], P('tp', 'sp'), may hold values from -0.25 to 0.25
Outputs:
- layer_out: bfloat16 [12288, 2048], P(('sp', 'tp'))
All inputs are finite; a program needn't handle non-finite values.
Results may differ from a plain program's by a relative error of at most 0.018.
The roundings to bfloat16 on the way count: a program that leaves them out, or rounds other values in their place, can miss the bound.
Values may be sent and summed in bfloat16 or wider, within the bound.
A program may use at most 64 MiB of HBM per device.

v0:
```python
import math

import jax
import jax.numpy as jnp
from jax import lax
from jax.sharding import Mesh
from jax.sharding import PartitionSpec as P

GRID_W = 128
SP = ("sp_0", "sp_1")
SP_TP = ("sp_0", "sp_1", "tp")


EPS = 1e-06
THETA = 10000.0


def side_by_side(arrays, axis, dim, along):
    ends, at = ([], 0)
    for a in arrays[:-1]:
        at += a.shape[along]
        ends.append(at)
    both = jnp.concatenate(arrays, axis=along)
    return tuple(jnp.split(lax.all_gather(both, axis, axis=dim, tiled=True), ends, axis=along))


def whole_of(value, axes, dim):
    for axis in reversed(axes):
        value = lax.all_gather(value, axis, axis=dim, tiled=True)
    return value


def in_blocks(value, dim, devices):
    dims = value.shape
    parts = value.reshape(*dims[:dim], devices, dims[dim] // devices, *dims[dim + 1 :])
    return jnp.moveaxis(parts, dim, 0)


def summed_on_arrival(value, axis, dim):
    parts = in_blocks(value, dim, lax.axis_size(axis))
    arrived = lax.all_to_all(parts, axis, split_axis=0, concat_axis=0, tiled=True)
    return arrived.astype(jnp.float32).sum(axis=0)


def in_order(parts, dim):
    parts = jnp.moveaxis(parts, 0, dim)
    dims = parts.shape
    return parts.reshape(*dims[:dim], dims[dim] * dims[dim + 1], *dims[dim + 2 :])


def copy_for_each(value, axis):
    devices = lax.axis_size(axis)
    return lax.all_to_all(
        jnp.broadcast_to(value[None], (devices, *value.shape)), axis, 0, 0, tiled=True
    )


def gather_directly(value, axis, dim):
    return in_order(copy_for_each(value, axis), dim)


def turn_half(part, angle):
    quarter = part.shape[-1] // 2
    cos_table = jnp.cos(angle)[:, None, :]
    sin_table = jnp.sin(angle)[:, None, :]
    first_part = part[..., :quarter]
    second_part = part[..., quarter:]
    return jnp.concatenate(
        [
            first_part * cos_table - second_part * sin_table,
            first_part * sin_table + second_part * cos_table,
        ],
        axis=-1,
    )


def head_norm_rope(flat, gain, offset, head_count):
    tok_rows = flat.shape[0]
    head_size = flat.shape[1] // head_count
    heads = flat.astype(jnp.float32).reshape(tok_rows, head_count, head_size)
    heads = heads * lax.rsqrt(jnp.mean(heads * heads, axis=-1, keepdims=True) + EPS) * gain
    positions = offset + jnp.arange(tok_rows, dtype=jnp.int32)
    row_pos = (positions // GRID_W).astype(jnp.float32)
    col_pos = (positions % GRID_W).astype(jnp.float32)
    half_size = head_size // 2
    inv_freq = THETA ** (-jnp.arange(0, half_size, 2, dtype=jnp.float32) / half_size)
    turned = jnp.concatenate(
        [
            turn_half(heads[..., :half_size], row_pos[:, None] * inv_freq[None, :]),
            turn_half(heads[..., half_size:], col_pos[:, None] * inv_freq[None, :]),
        ],
        axis=-1,
    )
    return turned.reshape(tok_rows, head_count * head_size).astype(jnp.bfloat16)


def body(queries, keys, values, q_gain, k_gain, w_out, residual, norm_gain, w_gate, w_up, w_down):
    tok_rows = queries.shape[0]
    head_size = q_gain.shape[0]
    q_heads = queries.shape[1] // head_size
    kv_heads = keys.shape[1] // head_size
    q_group = q_heads // kv_heads
    offset = lax.axis_index(SP) * tok_rows
    q_rot = head_norm_rope(queries, q_gain, offset, q_heads)
    k_rot = head_norm_rope(keys, k_gain, offset, kv_heads)
    gate_whole, up_whole = side_by_side((w_gate, w_up), SP, 0, 1)
    down_whole = whole_of(w_down, SP, 1)
    query_groups = q_rot.reshape(tok_rows, kv_heads, q_group, head_size)
    score_scale = head_size ** (-0.5)
    start_state = (
        jnp.full((kv_heads, q_group, tok_rows), -1e30, jnp.float32),
        jnp.zeros((kv_heads, q_group, tok_rows), jnp.float32),
        jnp.zeros((kv_heads, q_group, tok_rows, head_size), jnp.float32),
    )
    running = start_state
    key_piece, value_piece = side_by_side((k_rot, values), SP, 0, 1)
    piece_len = key_piece.shape[0]
    block_len = math.gcd(piece_len, 512)
    blocks = piece_len // block_len
    key_blocks = key_piece.reshape(blocks, block_len, kv_heads, head_size)
    value_blocks = value_piece.reshape(blocks, block_len, kv_heads, head_size)

    def update(state, block_pair):
        prior_max, totals, accum = state
        key_block, value_block = block_pair
        scores = (
            jnp.einsum(
                "qhgd,khd->hgqk", query_groups, key_block, preferred_element_type=jnp.float32
            )
            * score_scale
        )
        new_max = jnp.maximum(prior_max, jnp.max(scores, axis=-1))
        weights = jnp.exp(scores - new_max[..., None])
        factor = jnp.exp(prior_max - new_max)
        totals = totals * factor + jnp.sum(weights, axis=-1)
        accum = accum * factor[..., None] + jnp.einsum(
            "hgqk,khd->hgqd",
            weights.astype(jnp.bfloat16),
            value_block,
            preferred_element_type=jnp.float32,
        )
        return ((new_max, totals, accum), None)

    running, unused = lax.scan(update, running, (key_blocks, value_blocks))
    final_max, totals, accum = running
    mixed = accum / totals[..., None]
    attn = (
        jnp.transpose(mixed, (2, 0, 1, 3))
        .reshape(tok_rows, q_heads * head_size)
        .astype(jnp.bfloat16)
    )
    picked = attn
    proj = summed_on_arrival(
        jnp.dot(picked, w_out, preferred_element_type=jnp.float32).astype(jnp.bfloat16), "tp", 0
    )
    mid = residual.astype(jnp.float32) + proj
    normed = (
        mid * lax.rsqrt(jnp.mean(mid * mid, axis=-1, keepdims=True) + EPS) * norm_gain
    ).astype(jnp.bfloat16)
    gathered = gather_directly(normed, "tp", 0)
    gate = jnp.dot(gathered, gate_whole, preferred_element_type=jnp.float32)
    up_part = jnp.dot(gathered, up_whole, preferred_element_type=jnp.float32)
    hidden = (jax.nn.silu(gate) * up_part).astype(jnp.bfloat16)
    picked = hidden
    down = summed_on_arrival(
        jnp.dot(picked, down_whole, preferred_element_type=jnp.float32).astype(jnp.bfloat16),
        "tp",
        0,
    )
    return (mid + 0.5 * down).astype(jnp.bfloat16)


def solution(mesh):
    finer = Mesh(mesh.devices.reshape(16, 4, mesh.shape["tp"]), ("sp_0", "sp_1", "tp"))
    placed = (
        P(SP, "tp"),
        P(SP, "tp"),
        P(SP, "tp"),
        P(),
        P(),
        P("tp", None),
        P(SP_TP, None),
        P(),
        P(SP, "tp"),
        P(SP, "tp"),
        P("tp", SP),
    )
    return jax.shard_map(
        body, mesh=finer, in_specs=placed, out_specs=P(SP_TP, None), check_vma=False
    )
```

profile of v0, /device:TPU:1, one launch (start us, length us, event | category | flops | bytes accessed | tf_op | source)
XLA Modules:
  0.0 408.5 jit_solution(6992824680138517286)
XLA Ops:
  10.1 1.5 pad_maximum_fusion
  11.7 12.5 %all_gather.14 = bf16[704,128]{0,1:T(8,128)(2,1)} all-gather(bf16[704,32]{0,1:T(8,128)(2,1)} %param.23), channel_id=1, replica_groups=mesh['sp_0'=16,'sp_1'=4,'tp'=8] {'sp_1'}, dimensions={1}, use_global_device_ids=true | all-gather | bytes 225280 | tf_op jit(solution)/shard_map/all_gather | solution.py:29
  26.2 123.9 %all-gather.4.cloned.1.call-done = bf16[12288,128]{1,0:T(8,128)(2,1)} async-done(((bf16[192,128]{1,0:T(8,128)(2,1)}), bf16[12288,128]{1,0:T(8,128)(2,1)}) %all-gather.4.cloned.1.call-update) | async-done | bytes 3145744 | tf_op jit(solution)/shard_map/all_gather | solution.py:24
  150.0 6.2 %fusion.61 = (bf16[12288,64]{1,0:T(8,128)(2,1)}, bf16[12288,64]{1,0:T(8,128)(2,1)}) fusion(bf16[12288,128]{1,0:T(8,128)(2,1)} %all-gather.4.cloned.1.call-done), kind=kLoop, calls=%fused_computation.103 | loop fusion | bytes 6291456 | tf_op jit(solution)/shard_map/split | solution.py:24
  156.3 3.1 copy.27
  159.4 4.3 %copy.28 = bf16[24,512,1,64]{1,3,2,0:T(8,128)(2,1)} copy(bf16[24,512,1,64]{3,1,0,2:T(8,128)(2,1)} %bitcast.81) | data formatting | bytes 3145728
  163.7 48.3 %while.15 = (s32[]{:T(128)}, f32[1,2,192]{2,1,0:T(2,128)S(1)}, f32[1,2,192]{2,1,0:T(2,128)S(1)}, f32[1,2,192,64]{2,3,1,0:T(8,128)S(1)}, bf16[24,512,1,64]{1,3,2,...) while((s32[]{:T(128)}, f32[1,2,192]{2,1,0:T(2,128)S(1)}, ...), condition=%wide.region_5.6_spmd.clone, body=%wide.region_2.5_spmd.clone.sunk | while | flops 51587328 | bytes 2777709 | solution.py:144
  170.1 1.2 fusion.78
  172.1 1.2 fusion.78
  174.2 1.2 fusion.78
  176.2 1.2 fusion.78
  178.2 1.2 fusion.78
  180.2 1.2 fusion.78
  182.2 1.2 fusion.78
  184.2 1.2 fusion.78
  186.2 1.2 fusion.78
  188.2 1.2 fusion.78
  190.3 1.2 fusion.78
  192.3 1.2 fusion.78
  194.3 1.2 fusion.78
  196.3 1.2 fusion.78
  198.3 1.2 fusion.78
  200.3 1.2 fusion.78
  204.3 1.2 fusion.78
  208.4 1.2 fusion.78
  212.4 25.6 %all_to_all.15 = bf16[8,24,2048]{2,1,0:T(8,128)(2,1)S(1)} all-to-all(bf16[8,24,2048]{2,1,0:T(8,128)(2,1)S(1)} %bitcast.83), channel_id=1, replica_groups=mesh['sp_0'=16,'sp_1'=4,'tp'=8] {'tp'}, dimensions={0} | all-to-all | bytes 1572864 | tf_op jit(solution)/shard_map/all_to_all | solution.py:41
  238.5 15.6 %all_to_all.16 = bf16[8,24,2048]{2,1,0:T(8,128)(2,1)S(1)} all-to-all(bf16[8,24,2048]{2,1,0:T(8,128)(2,1)S(1)} %broadcast_in_dim.11), channel_id=1, replica_groups=mesh['sp_0'=16,'sp_1'=4,'tp'=8] {'tp'}, dimensions={0} | all-to-all | bytes 1572864 | tf_op jit(solution)/shard_map/all_to_all | solution.py:53
  254.1 44.4 %all-gather.6.cloned.1.call-done = bf16[2048,1408]{1,0:T(8,128)(2,1)} async-done(((bf16[32,1408]{1,0:T(8,128)(2,1)}), bf16[2048,1408]{1,0:T(8,128)(2,1)}) %all-gather.6.cloned.1.call-update) | async-done | bytes 5767184 | tf_op jit(solution)/shard_map/all_gather | solution.py:24
  298.5 2.7 fusion.17
  301.2 69.2 %all-gather.8.cloned.1.call-done = bf16[704,2048]{0,1:T(8,128)(2,1)} async-done(((bf16[704,128]{0,1:T(8,128)(2,1)}), bf16[704,2048]{0,1:T(8,128)(2,1)}) %all-gather.8.cloned.1.call-update) | async-done | bytes 2883600 | tf_op jit(solution)/shard_map/all_gather | solution.py:29
  370.4 5.0 %convolution_convert_fusion = bf16[192,2048]{1,0:T(8,128)(2,1)S(1)} fusion(bf16[704,2048]{0,1:T(8,128)(2,1)} %all-gather.8.cloned.1.call-done, bf16[192,2048]{1,0:T(8,128)(2,1)S(1)} %bitcast.87, bf16[2048,1408]{1,0:T(8,128)(2,1)} %all-gather.6.cloned.1.call-done, f32[192,704]{1,0:T(8,128)S(1)} %fusion.17), kind=kOutput, calls=%fused_computation.27 | convolution fusion | flops 1108500480 | bytes 8404992 | tf_op jit(solution)/shard_map/dot_general | solution.py:166
  375.4 25.8 %all_to_all.17 = bf16[8,24,2048]{2,1,0:T(8,128)(2,1)S(1)} all-to-all(bf16[8,24,2048]{2,1,0:T(8,128)(2,1)S(1)} %bitcast.88), channel_id=1, replica_groups=mesh['sp_0'=16,'sp_1'=4,'tp'=8] {'tp'}, dimensions={0} | all-to-all | bytes 1572864 | tf_op jit(solution)/shard_map/all_to_all | solution.py:41
  (166 shorter events, 32.3 us)
Async XLA Ops:
  6.5 205.5 %copy-start = (bf16[128,2048]{1,0:T(8,128)(2,1)S(1)}, bf16[128,2048]{1,0:T(8,128)(2,1)}, u32[]{:S(2)}) copy-start(bf16[128,2048]{1,0:T(8,128)(2,1)} %param.18) | copy-start | bytes 1572868
  6.5 143.5 %all-gather.4.cloned.1.call-start = ((), (), s32[]{:S(2)}) async-start(), calls=%async_computation.3 | async-start | bytes 3194880 | tf_op jit(solution)/shard_map/all_gather | solution.py:24
  10.0 288.5 %all-gather.6.cloned.1.call-start = ((), (), s32[]{:S(2)}) async-start(), calls=%async_computation.4 | async-start | bytes 5857280 | tf_op jit(solution)/shard_map/all_gather | solution.py:24
  11.6 358.8 %all-gather.8.cloned.1.call-start = ((), (), s32[]{:S(2)}) async-start(), calls=%async_computation.5 | async-start | bytes 3342336 | tf_op jit(solution)/shard_map/all_gather | solution.py:29
  212.0 26.2 %copy-start.1 = (bf16[24,2048]{1,0:T(8,128)(2,1)S(1)}, bf16[24,2048]{1,0:T(8,128)(2,1)}, u32[]{:S(2)}) copy-start(bf16[24,2048]{1,0:T(8,128)(2,1)} %param.19) | copy-start | bytes 294916
  212.0 26.4 %copy-start.2 = (f32[2048]{0:T(1024)S(1)}, f32[2048]{0:T(1024)}, u32[]{:S(2)}) copy-start(f32[2048]{0:T(1024)} %param.20) | copy-start | bytes 24580
Sparse Core Ops, SparseCore 0:
  10.3 139.7 all-gather.3
  153.0 145.4 all-gather.5
  300.6 69.7 all-gather.7
where the time goes:
time: 410 us; the launch traced here: 408 us
  waiting for transfers between devices  238 us (58%)
  blocking collectives  79.5 us (19%)
  matrix products  47.4 us (12%)
  local copies, waits for them, and re-layouts  15.4 us (4%)
  other arithmetic  14.3 us (3%)
  between operations  13.3 us (3%)
    all_gather x2, waiting for transfers between devices, side_by_side(): lax.all_gather(both, axis, axis=dim, tiled=True)  168 us
    all_gather x1, waiting for transfers between devices, whole_of(): value = lax.all_gather(value, axis, axis=dim, tiled=True)  69.2 us
    all_to_all x2, blocking collectives, summed_on_arrival(): lax.all_to_all(parts, axis, split_axis=0, concat_axis=0, tiled=True)  51.4 us
    dot_general x24, matrix products, update(): jnp.einsum('hgqk,khd->hgqd', weights.astype(jnp.bfloat16), value_block, p...  29.3 us
    all_to_all x1, blocking collectives, copy_for_each(): lax.all_to_all(jnp.broadcast_to(value[None], (devices, *value.shape)), ax...  15.6 us
    all_gather x1, blocking collectives, whole_of(): value = lax.all_gather(value, axis, axis=dim, tiled=True)  12.5 us
    dot_general x24, matrix products, update(): jnp.einsum('qhgd,khd->hgqk', query_groups, key_block, preferred_element_t...  10 us
  transfers between devices with their start and end apart: 3, of which 3 were waited for; matrix products, arithmetic and copies ran while one was open for 17% of the time, Pallas kernels for 0%

commit v1 on v0

v1 whole, which is shorter than its diff:
```python
import jax
import jax.numpy as jnp
from jax import lax
from jax.experimental import pallas as pl
from jax.experimental.pallas import tpu as pltpu
from jax.sharding import Mesh
from jax.sharding import PartitionSpec as P

GRID_W = 128
EPS = 1e-06
THETA = 10000.0
NZ, NY, NX, NC = 16, 4, 4, 2
TOK = 192
ROWS = 24
DM = 2048
HID = 704
UNITS = HID // NY
F32 = jnp.float32
BF16 = jnp.bfloat16
PARTS = ((0, 272), (272, 256))


def nt(a, b):
    return lax.dot_general(a, b, (((1,), (1,)), ((), ())), preferred_element_type=F32)


def norm_rope(h, gain, tab):
    n = h * lax.rsqrt(jnp.mean(h * h, axis=0, keepdims=True) + EPS) * gain
    cr, sr, cc, sc = tab[0:16], tab[16:32], tab[32:48], tab[48:64]
    a, b, c, d = n[0:16], n[16:32], n[32:48], n[48:64]
    return jnp.concatenate([a * cr - b * sr, a * sr + b * cr, c * cc - d * sc, c * sc + d * cc], axis=0)


def kernel(
    q_ref, kt_ref, vt_ref, tab_ref, wg_ref, wu_ref, wdt_ref, wout_ref, res_ref, ng_ref, out_ref,
    kv, qa, kk, vv, mx0, mx1, ls0, ls1, acc, wt, wp, ws, wm, wo, rs_, aa, osend, orecv, ssend, srecv,
    mid, nb, dn, pown, dsend, drecv, rsend, rrecv, mown, osum,
    kvs, kvr, qs, qr, wps, wpr, wrs, wrr, r1s, r1r, r2s, r2r, rds, rdr, wos, wor, wds, wdr,
    os_, or_, ss_, sr_, as_, ar_, ads, adr, dds, ddr, fs, fr,
):
    z, y, x, c = (lax.axis_index(n) for n in ("z", "y", "x", "c"))
    tp = x * 2 + c
    pending = []

    def go(src, dst, ssem, rsem, dev):
        cp = pltpu.make_async_remote_copy(
            src_ref=src, dst_ref=dst, send_sem=ssem, recv_sem=rsem, device_id=dev, device_id_type=pl.DeviceIdType.MESH
        )
        cp.start()
        pending.append(cp)

    def got(dst, ssem, rsem):
        pltpu.make_async_remote_copy(
            src_ref=dst, dst_ref=dst, send_sem=ssem, recv_sem=rsem, device_id=(z, y, x, c), device_id_type=pl.DeviceIdType.MESH
        ).wait_recv()

    def up(v, d, n):
        return lax.rem(v + d + n, n)

    def lanes(i):
        return pl.ds(pl.multiple_of(i * 128, 128), 128)

    partner = (z, y, x, 1 - c)
    znext, zprev = (up(z, 1, NZ), y, x, c), (up(z, -1, NZ), y, x, c)

    bar = pltpu.get_barrier_semaphore()
    peers = [partner, znext, zprev]
    for d in range(NY):
        for e in range(NX):
            if d or e:
                peers.append((z, up(y, d, NY), up(x, e, NX), c))
    for p in peers:
        pl.semaphore_signal(bar, inc=1, device_id=p, device_id_type=pl.DeviceIdType.MESH)

    tab = tab_ref[...]
    kr = norm_rope(kt_ref[...].astype(F32), tab[128:192], tab)
    kv[0] = jnp.concatenate([kr, vt_ref[...].astype(F32)], axis=0).T.astype(BF16)
    qt = q_ref[...].astype(F32).T
    qr2 = jnp.concatenate([norm_rope(qt[0:64], tab[64:128], tab), norm_rope(qt[64:128], tab[64:128], tab)], axis=0)
    qa[y] = (qr2.T * 0.125).astype(BF16)
    w4 = jnp.concatenate(
        [wg_ref[...].astype(F32), wu_ref[...].astype(F32), wdt_ref[...].astype(F32), jnp.zeros((32, HID), F32)], axis=0
    )
    wt[...] = w4.T
    for d in range(NY):
        yb = up(y, d, NY)
        piece = wt[pl.ds(pl.multiple_of(yb * UNITS, 8), UNITS), :].astype(BF16)
        if d == 0:
            wp[y] = piece
        else:
            ws[d - 1] = piece
    pl.semaphore_wait(bar, len(peers))

    def kv_cw(s):
        go(kv.at[0 if s == 0 else 2 * s - 1], kv.at[2 * s + 1], kvs.at[0, s], kvr.at[0, s], znext)

    def kv_ccw(s):
        go(kv.at[2 * s], kv.at[2 * s + 2], kvs.at[1, s], kvr.at[1, s], zprev)

    kv_cw(0)
    kv_ccw(0)
    for d in range(1, NY):
        dev = (z, up(y, d, NY), x, c)
        go(qa.at[y], qa.at[y], qs.at[d - 1], qr.at[d - 1], dev)
    for d in range(1, NY):
        dev = (z, up(y, d, NY), x, c)
        go(ws.at[d - 1], wp.at[y], wps.at[d - 1], wpr.at[d - 1], dev)
    for e in range(1, NX):
        dev = (z, y, up(x, e, NX), c)
        go(res_ref, rs_.at[c, y, x], r1s.at[e - 1], r1r.at[e - 1], dev)
    wrow = pl.ds(pl.multiple_of(tp * 128, 128), 128)
    for e in range(1, NX):
        dev = (z, y, up(x, e, NX), c)
        go(wout_ref, wo.at[wrow], wos.at[e - 1], wor.at[e - 1], dev)
    go(wout_ref, wo.at[wrow], wds.at[0], wdr.at[0], partner)
    wo[wrow] = wout_ref[...]
    rs_[c, y, x] = res_ref[...]

    def w_slice(part, blk):
        r0, nr = PARTS[part]
        return wm.at[pl.ds(r0, nr), lanes(blk)]

    def w_send(part, j, way):
        sl = w_slice(part, up(z, -j if way == 0 else j, NZ))
        go(sl, sl, wrs.at[way, part, j], wrr.at[way, part, j], znext if way == 0 else zprev)

    def pump(t):
        part, j = t % 2, t // 2
        for way, last in ((0, 8), (1, 7)):
            if j < last:
                sl = w_slice(part, up(z, -1 - j if way == 0 else 1 + j, NZ))
                got(sl, wrs.at[way, part, j], wrr.at[way, part, j])
                if j + 1 < last:
                    w_send(part, j + 1, way)

    lane = lax.broadcasted_iota(jnp.int32, (UNITS, 128), 1)

    def w_start():
        for d in range(1, NY):
            got(wp.at[up(y, -d, NY)], wps.at[d - 1], wpr.at[d - 1])
        pieces = [wp[i].astype(F32) for i in range(NY)]
        for m in range(3):
            blk = None
            for i in range(NY):
                sh = (32 * (i - m)) % 128
                r = pltpu.roll(pieces[i], sh, 1) if sh else pieces[i]
                blk = r if blk is None else jnp.where(lane >= 32 * i, r, blk)
            wm[pl.ds(m * UNITS, UNITS), lanes(z)] = blk.astype(BF16)
        for part in range(2):
            w_send(part, 0, 0)
            w_send(part, 0, 1)

    for d in range(1, NY):
        got(qa.at[up(y, -d, NY)], qs.at[d - 1], qr.at[d - 1])
    mx0[...] = jnp.full(mx0.shape, -1e30, F32)
    mx1[...] = jnp.full(mx1.shape, -1e30, F32)
    ls0[...] = jnp.zeros(ls0.shape, F32)
    ls1[...] = jnp.zeros(ls1.shape, F32)
    acc[...] = jnp.zeros(acc.shape, F32)

    low = lax.broadcasted_iota(jnp.int32, (2 * TOK, 128), 1) < 64
    clow = lax.broadcasted_iota(jnp.int32, (128, 128), 1) < 64

    def attend(s):
        both = jnp.concatenate([kv[2 * s], kv[2 * s + 1]], axis=0).astype(F32)
        turned = pltpu.roll(both, 64, 1)
        none = jnp.zeros_like(both)
        kk[0 : 2 * TOK] = jnp.where(low, both, none).astype(BF16)
        kk[2 * TOK : 4 * TOK] = jnp.where(low, none, turned).astype(BF16)
        vv[0 : 2 * TOK] = jnp.where(low, turned, none).astype(BF16)
        vv[2 * TOK : 4 * TOK] = jnp.where(low, none, both).astype(BF16)

        def chunk(i, carry):
            yb = i // 3
            rows = pl.ds(pl.multiple_of(i * 64, 64), 64)
            sub = pl.ds(pl.multiple_of((i - 3 * yb) * 64, 64), 64)
            sc = nt(qa[yb, sub], kk[...])
            probs, facs = [], []
            for h, (mx, ls) in enumerate(((mx0, ls0), (mx1, ls1))):
                cols = [sc[:, 128 * (3 * h + j) : 128 * (3 * h + j + 1)] for j in range(3)]
                old = mx[rows]
                top = jnp.max(jnp.maximum(jnp.maximum(cols[0], cols[1]), cols[2]), axis=1, keepdims=True)
                new = jnp.maximum(old, top)
                fac = jnp.exp(old - new)
                ps = [jnp.exp(v - new) for v in cols]
                ls[rows] = ls[rows] * fac + (ps[0] + ps[1] + ps[2])
                mx[rows] = new
                probs += ps
                facs.append(fac)
            pb = jnp.concatenate([p.astype(BF16) for p in probs], axis=1)
            o = jnp.dot(pb, vv[...], preferred_element_type=F32)
            acc[rows] = acc[rows] * jnp.where(clow[0:64], facs[0], facs[1]) + o
            return carry

        lax.fori_loop(0, 12, chunk, 0)

    for s in range(8):
        got(kv.at[2 * s + 1], kvs.at[0, s], kvr.at[0, s])
        if s < 7:
            kv_cw(s + 1)
            got(kv.at[2 * s + 2], kvs.at[1, s], kvr.at[1, s])
            if s < 6:
                kv_ccw(s + 1)
        if s == 1:
            w_start()
        if s >= 3:
            pump(s - 3)
        if s == 3:
            for e in range(1, NX):
                got(rs_.at[c, y, up(x, -e, NX)], r1s.at[e - 1], r1r.at[e - 1])
            for d in range(1, NY):
                go(rs_.at[c, y], rs_.at[c, y], r2s.at[d - 1], r2r.at[d - 1], (z, up(y, d, NY), x, c))
            go(rs_.at[c, y], rs_.at[c, y], rds.at[0], rdr.at[0], partner)
        attend(s)

    lane_t = lax.broadcasted_iota(jnp.int32, (TOK, 128), 1)
    tlow = lane_t < 64
    thalf = lax.rem(lane_t, 64) < 32

    def part_of(yb):
        rows = pl.ds(pl.multiple_of(yb * TOK, 64), TOK)
        l0 = jnp.sum(ls0[rows], axis=1, keepdims=True)
        l1 = jnp.sum(ls1[rows], axis=1, keepdims=True)
        lb = jnp.where(tlow, l0, l1)
        mb = jnp.where(tlow, mx0[rows], mx1[rows])
        st = jnp.where(thalf, mb, lb).T
        packed = jnp.concatenate([st[0:8], st[32:40], st[64:72], st[96:104]], axis=0)
        return acc[rows] / lb, packed

    for d in range(1, NY):
        yb = up(y, d, NY)
        o, st = part_of(yb)
        osend[d - 1] = o.astype(BF16)
        ssend[d - 1] = st
        dev = (z, yb, x, c)
        go(ssend.at[d - 1], srecv.at[d - 1], ss_.at[d - 1], sr_.at[d - 1], dev)
        go(osend.at[d - 1], orecv.at[d - 1], os_.at[d - 1], or_.at[d - 1], dev)
    pump(5)
    mine, st = part_of(y)
    outs, stats = [mine], [st]
    for d in range(1, NY):
        got(srecv.at[d - 1], ss_.at[d - 1], sr_.at[d - 1])
        got(orecv.at[d - 1], os_.at[d - 1], or_.at[d - 1])
        outs.append(orecv[d - 1].astype(F32))
        stats.append(srecv[d - 1])
    coef = []
    for h in range(2):
        ms = [s_[16 * h : 16 * h + 8] for s_ in stats]
        top = jnp.maximum(jnp.maximum(ms[0], ms[1]), jnp.maximum(ms[2], ms[3]))
        wts = [s_[16 * h + 8 : 16 * h + 16] * jnp.exp(m - top) for s_, m in zip(stats, ms)]
        tot = (wts[0] + wts[1]) + (wts[2] + wts[3])
        coef.append([w / tot for w in wts])
    attn = None
    for p in range(NY):
        cf = jnp.concatenate([coef[0][p]] * 8 + [coef[1][p]] * 8, axis=0).T
        attn = cf * outs[p] if attn is None else attn + cf * outs[p]

    own = aa.at[y, :, lanes(tp)]
    aa[y, :, lanes(tp)] = attn.astype(BF16)
    for d in range(NY):
        for e in range(NX):
            o = d * NX + e
            if o:
                go(own, own, as_.at[o], ar_.at[o], (z, up(y, d, NY), up(x, e, NX), c))
    go(own, own, ads.at[0], adr.at[0], partner)

    for e in range(1, NX):
        wr = pl.ds(pl.multiple_of((up(x, -e, NX) * 2 + c) * 128, 128), 128)
        got(wo.at[wr], wos.at[e - 1], wor.at[e - 1])
        go(wo.at[wr], wo.at[wr], wds.at[e], wdr.at[e], partner)
    for d in range(1, NY):
        yb = up(y, -d, NY)
        got(rs_.at[c, yb], r2s.at[d - 1], r2r.at[d - 1])
        go(rs_.at[c, yb], rs_.at[c, yb], rds.at[d], rdr.at[d], partner)
    for t in range(6, 10):
        pump(t)
    for d in range(NY):
        for e in range(NX):
            o = d * NX + e
            if o:
                sl = aa.at[up(y, -d, NY), :, lanes(up(x, -e, NX) * 2 + c)]
                got(sl, as_.at[o], ar_.at[o])
                go(sl, sl, ads.at[o], adr.at[o], partner)
    for t in range(10, 16):
        pump(t)
    for e in range(NX):
        wr = pl.ds(pl.multiple_of((up(x, -e, NX) * 2 + 1 - c) * 128, 128), 128)
        got(wo.at[wr], wds.at[e], wdr.at[e])

    gain = ng_ref[...]

    def block(d):
        yb = up(y, -d, NY)
        for e in range(NX):
            sl = aa.at[yb, :, lanes(up(x, -e, NX) * 2 + 1 - c)]
            got(sl, ads.at[d * NX + e], adr.at[d * NX + e])
        got(rs_.at[1 - c, yb], rds.at[d], rdr.at[d])
        for n in range(4):
            cols = slice(512 * n, 512 * n + 512)
            mid[:, cols] = jnp.dot(aa[yb], wo[:, cols], preferred_element_type=F32)
        for t in range(8):
            r = slice(ROWS * t, ROWS * t + ROWS)
            v = mid[r] + rs_[t % 2, yb, t // 2].astype(F32)
            mid[r] = v
            sq = jnp.mean(v * v, axis=1, keepdims=True)
            dn[r] = v * lax.rsqrt(sq + EPS) * gain
        nb[...] = dn[...].astype(BF16)
        if d == 0:
            mown[...] = mid[pl.ds(pl.multiple_of(tp * ROWS, 8), ROWS)]
        g = nt(nb[...], wm[0:UNITS])
        u = nt(nb[...], wm[UNITS : 2 * UNITS])
        hid = (g / (1.0 + jnp.exp(-g)) * u).astype(BF16)
        for n in range(4):
            cols = slice(512 * n, 512 * n + 512)
            dn[:, cols] = jnp.dot(hid, wm[2 * UNITS : 3 * UNITS, cols], preferred_element_type=F32)
        for e in range(NX):
            xb = up(x, -e, NX)
            pown[d * NX + e] = dn[pl.ds(pl.multiple_of((xb * 2 + c) * ROWS, 8), ROWS)]
            dsend[d, e] = dn[pl.ds(pl.multiple_of((xb * 2 + 1 - c) * ROWS, 8), ROWS)].astype(BF16)
        go(dsend.at[d], drecv.at[d], dds.at[d], ddr.at[d], partner)

    def finish(d):
        got(drecv.at[d], dds.at[d], ddr.at[d])
        for e in range(NX):
            o = d * NX + e
            v = pown[o] + drecv[d, e].astype(F32)
            if o == 0:
                osum[...] = v
            else:
                rsend[o] = v.astype(BF16)
                go(rsend.at[o], rrecv.at[o], fs.at[o], fr.at[o], (z, up(y, -d, NY), up(x, -e, NX), c))

    for d in range(NY):
        block(d)
        if d:
            finish(d - 1)
    finish(NY - 1)
    total = osum[...]
    for o in range(1, NX * NY):
        got(rrecv.at[o], fs.at[o], fr.at[o])
        total = total + rrecv[o].astype(F32)
    out_ref[...] = (mown[...] + 0.5 * total).astype(BF16)
    for cp in pending:
        cp.wait_send()


def body(queries, keys, values, q_gain, k_gain, w_out, residual, norm_gain, w_gate, w_up, w_down):
    first = (lax.axis_index("z") * NY + lax.axis_index("y")) * TOK
    positions = first + jnp.arange(TOK, dtype=jnp.int32)
    row_pos = (positions // GRID_W).astype(F32)
    col_pos = (positions % GRID_W).astype(F32)
    inv_freq = THETA ** (-jnp.arange(0, 32, 2, dtype=F32) / 32)
    ar = inv_freq[:, None] * row_pos[None, :]
    ac = inv_freq[:, None] * col_pos[None, :]
    tab = jnp.concatenate(
        [
            jnp.cos(ar), jnp.sin(ar), jnp.cos(ac), jnp.sin(ac),
            jnp.broadcast_to(q_gain[:, None], (64, TOK)),
            jnp.broadcast_to(k_gain[:, None], (64, TOK)),
        ],
        axis=0,
    )
    v = pltpu.VMEM
    dma = pltpu.SemaphoreType.DMA
    scratch = [
        v((NZ, TOK, 128), BF16),
        v((NY, TOK, 128), BF16),
        v((4 * TOK, 128), BF16),
        v((4 * TOK, 128), BF16),
        *[v((NY * TOK, 128), F32)] * 5,
        v((HID, 128), F32),
        v((NY, UNITS, 128), BF16),
        v((NY - 1, UNITS, 128), BF16),
        v((3 * UNITS, DM), BF16),
        v((1024, DM), BF16),
        v((NC, NY, NX, ROWS, DM), BF16),
        v((NY, TOK, 1024), BF16),
        v((3, TOK, 128), BF16), v((3, TOK, 128), BF16),
        v((3, 32, TOK), F32), v((3, 32, TOK), F32),
        v((TOK, DM), F32), v((TOK, DM), BF16), v((TOK, DM), F32),
        v((16, ROWS, DM), F32),
        v((NY, NX, ROWS, DM), BF16), v((NY, NX, ROWS, DM), BF16),
        v((16, ROWS, DM), BF16), v((16, ROWS, DM), BF16),
        v((ROWS, DM), F32), v((ROWS, DM), F32),
        dma((2, 8)), dma((2, 8)), dma((3,)), dma((3,)), dma((3,)), dma((3,)), dma((2, 2, 8)), dma((2, 2, 8)),
        dma((3,)), dma((3,)), dma((3,)), dma((3,)), dma((4,)), dma((4,)), dma((3,)), dma((3,)), dma((4,)), dma((4,)),
        dma((3,)), dma((3,)), dma((3,)), dma((3,)), dma((16,)), dma((16,)), dma((16,)), dma((16,)),
        dma((4,)), dma((4,)), dma((16,)), dma((16,)),
    ]
    return pl.pallas_call(
        kernel,
        out_shape=jax.ShapeDtypeStruct((ROWS, DM), BF16),
        in_specs=[pl.BlockSpec(memory_space=pltpu.VMEM)] * 10,
        out_specs=pl.BlockSpec(memory_space=pltpu.VMEM),
        scratch_shapes=scratch,
        compiler_params=pltpu.CompilerParams(collective_id=0, has_side_effects=True, vmem_limit_bytes=60 * 1024 * 1024),
        name="layer",
    )(queries, keys.T, values.T, tab, w_gate, w_up, w_down.T, w_out, residual, norm_gain[None, :])


def solution(mesh):
    finer = Mesh(mesh.devices.reshape(NZ, NY, NX, NC), ("z", "y", "x", "c"))
    sp, tp, every = ("z", "y"), ("x", "c"), ("z", "y", "x", "c")
    placed = (
        P(sp, tp), P(sp, tp), P(sp, tp), P(), P(), P(tp, None), P(every, None), P(), P(sp, tp), P(sp, tp), P(tp, sp),
    )
    return jax.shard_map(body, mesh=finer, in_specs=placed, out_specs=P(every, None), check_vma=False)
```

time: 410 us -> 122 us (0.30)
  waiting for transfers between devices: 238 us -> 0 us
  Pallas kernels: 0 us -> 118 us
  blocking collectives: 79.5 us -> 0 us
  matrix products: 47.4 us -> 0 us
  other arithmetic: 14.3 us -> 0.58 us
  between operations: 13.3 us -> 0.04 us
  local copies, waits for them, and re-layouts: 15.4 us -> 3.45 us
    all_gather x3 -> x0, waiting for transfers between devices: 237 us -> none  [the longest x2 168 us: side_by_side(): lax.all_gather(both, axis, axis=dim, tiled=True)]
    pallas_call x0 -> x1, Pallas kernels: none -> 118 us  [body(): pl.pallas_call(kernel, out_shape=jax.ShapeDtypeStruct((ROWS, DM), BF16),...]
    all_to_all x3 -> x0, blocking collectives: 67 us -> none  [the longest x2 51.4 us: summed_on_arrival(): lax.all_to_all(parts, axis, split_axis=0, concat_axis=0, tiled=True)]
    dot_general x51 -> x0, matrix products: 47.4 us -> none  [the longest x24 29.3 us: update(): jnp.einsum('hgqk,khd->hgqd', weights.astype(jnp.bfloat16), value_block, p...]
    all_gather x1 -> x0, blocking collectives: 12.5 us -> none  [whole_of(): value = lax.all_gather(value, axis, axis=dim, tiled=True)]
    reduce_sum x29 -> x0, other arithmetic: 8.37 us -> none  [the longest x24 7.15 us: update(): totals = totals * factor + jnp.sum(weights, axis=-1)]
    split x1 -> x0, local copies, waits for them, and re-layouts: 6.21 us -> none  [side_by_side(): jnp.split(lax.all_gather(both, axis, axis=dim, tiled=True), ends, axis=al...]
  transfers between devices with their start and end apart: 3 -> 0, of which waited for: 3 -> 0; matrix products, arithmetic and copies ran while one was open for 17% -> 0% of each run, Pallas kernels for 0% -> 0%
where the time goes in v1:
time: 122 us
  Pallas kernels  118 us (97%)
  local copies, waits for them, and re-layouts  3.45 us (3%)
    pallas_call x1, Pallas kernels, body(): pl.pallas_call(kernel, out_shape=jax.ShapeDtypeStruct((ROWS, DM), BF16),...  118 us
    unnamed x8, local copies, waits for them, and re-layouts  3.38 us

profile of v1, /device:TPU:1, one launch (start us, length us, event | category | flops | bytes accessed | tf_op | source)
XLA Modules:
  0.0 122.2 jit_solution(15892432411442129621)
XLA Ops:
  0.0 0.1 fusion
  0.2 0.1 fusion.1
  0.3 0.1 fusion.2
  0.5 0.0 copy-start.1
  0.5 0.1 fusion.3
  0.6 0.5 copy-done.1
  1.1 0.0 copy-start.2
  1.1 0.1 broadcast_dynamic-update-slice_fusion.1
  1.2 0.6 copy-done.2
  1.8 0.1 broadcast_dynamic-update-slice_fusion.tab_ref
  1.8 0.0 copy-start
  1.8 0.7 copy-done
  2.5 118.2 %layer.1 = bf16[24,2048]{1,0:T(8,128)(2,1)} custom-call(bf16[192,128]{1,0:T(8,128)(2,1)} %q_ref.1, bf16[64,192]{1,0:T(8,128)(2,1)} %bitcast.5, bf16[64,192]{1,0:T(8,128)(2,1)} %bitcast.6, f32[192,192]{1,0:T(8,128)} %copy-done, bf16[32,704]{1,0:T(8,128)(2,1)} %wg_ref.1, bf16[32,704]{1,0:T(8,128)(2,1)} %wu_ref.1, bf16[32,704]{1,0:T(8,128)(2,1)} %bitcast.4, ...), custom_call_target="tpu_custom_call" | custom-call | tf_op jit(solution)/shard_map/layer/pallas_call | solution.py:390
  120.7 1.5 %copy.18 = bf16[24,2048]{1,0:T(8,128)(2,1)} copy(bf16[24,2048]{1,0:T(8,128)(2,1)} %layer.1) | data formatting | bytes 196608
  (2 shorter events, 0.0 us)
Async XLA Ops:
  0.5 0.7 copy-start.1
  1.1 0.7 copy-start.2
  1.8 0.7 copy-start

commit v2 on v1

--- a/solution.py
+++ b/solution.py
@@ -17,7 +17,7 @@
 UNITS = HID // NY
 F32 = jnp.float32
 BF16 = jnp.bfloat16
-PARTS = ((0, 272), (272, 256))
+PARTS = tuple((UNITS * m, UNITS) for m in range(3))
 
 
 def nt(a, b):
@@ -34,9 +34,9 @@
 def kernel(
     q_ref, kt_ref, vt_ref, tab_ref, wg_ref, wu_ref, wdt_ref, wout_ref, res_ref, ng_ref, out_ref,
     kv, qa, kk, vv, mx0, mx1, ls0, ls1, acc, wt, wp, ws, wm, wo, rs_, aa, osend, orecv, ssend, srecv,
-    mid, nb, dn, pown, dsend, drecv, rsend, rrecv, mown, osum,
+    mid, nb, dn, pown, dsend, drecv, mown, asend, arecv, aown, bsend, brecv, bown, a2send, a2recv, b2send, b2recv, outa,
     kvs, kvr, qs, qr, wps, wpr, wrs, wrr, r1s, r1r, r2s, r2r, rds, rdr, wos, wor, wds, wdr,
-    os_, or_, ss_, sr_, as_, ar_, ads, adr, dds, ddr, fs, fr,
+    os_, or_, ss_, sr_, as_, ar_, ads, adr, dds, ddr, f1s, f1r, f2s, f2r, f3s, f3r, f4s, f4r,
 ):
     z, y, x, c = (lax.axis_index(n) for n in ("z", "y", "x", "c"))
     tp = x * 2 + c
@@ -125,7 +125,7 @@
         go(sl, sl, wrs.at[way, part, j], wrr.at[way, part, j], znext if way == 0 else zprev)
 
     def pump(t):
-        part, j = t % 2, t // 2
+        part, j = t % 3, t // 3
         for way, last in ((0, 8), (1, 7)):
             if j < last:
                 sl = w_slice(part, up(z, -1 - j if way == 0 else 1 + j, NZ))
@@ -146,12 +146,10 @@
                 r = pltpu.roll(pieces[i], sh, 1) if sh else pieces[i]
                 blk = r if blk is None else jnp.where(lane >= 32 * i, r, blk)
             wm[pl.ds(m * UNITS, UNITS), lanes(z)] = blk.astype(BF16)
-        for part in range(2):
+        for part in range(3):
             w_send(part, 0, 0)
             w_send(part, 0, 1)
 
-    for d in range(1, NY):
-        got(qa.at[up(y, -d, NY)], qs.at[d - 1], qr.at[d - 1])
     mx0[...] = jnp.full(mx0.shape, -1e30, F32)
     mx1[...] = jnp.full(mx1.shape, -1e30, F32)
     ls0[...] = jnp.zeros(ls0.shape, F32)
@@ -159,7 +157,7 @@
     acc[...] = jnp.zeros(acc.shape, F32)
 
     low = lax.broadcasted_iota(jnp.int32, (2 * TOK, 128), 1) < 64
-    clow = lax.broadcasted_iota(jnp.int32, (128, 128), 1) < 64
+    qlow = lax.broadcasted_iota(jnp.int32, (NY * TOK, 128), 1) < 64
 
     def attend(s):
         both = jnp.concatenate([kv[2 * s], kv[2 * s + 1]], axis=0).astype(F32)
@@ -170,29 +168,22 @@
         vv[0 : 2 * TOK] = jnp.where(low, turned, none).astype(BF16)
         vv[2 * TOK : 4 * TOK] = jnp.where(low, none, both).astype(BF16)
 
-        def chunk(i, carry):
-            yb = i // 3
-            rows = pl.ds(pl.multiple_of(i * 64, 64), 64)
-            sub = pl.ds(pl.multiple_of((i - 3 * yb) * 64, 64), 64)
-            sc = nt(qa[yb, sub], kk[...])
-            probs, facs = [], []
-            for h, (mx, ls) in enumerate(((mx0, ls0), (mx1, ls1))):
-                cols = [sc[:, 128 * (3 * h + j) : 128 * (3 * h + j + 1)] for j in range(3)]
-                old = mx[rows]
-                top = jnp.max(jnp.maximum(jnp.maximum(cols[0], cols[1]), cols[2]), axis=1, keepdims=True)
-                new = jnp.maximum(old, top)
-                fac = jnp.exp(old - new)
-                ps = [jnp.exp(v - new) for v in cols]
-                ls[rows] = ls[rows] * fac + (ps[0] + ps[1] + ps[2])
-                mx[rows] = new
-                probs += ps
-                facs.append(fac)
-            pb = jnp.concatenate([p.astype(BF16) for p in probs], axis=1)
-            o = jnp.dot(pb, vv[...], preferred_element_type=F32)
-            acc[rows] = acc[rows] * jnp.where(clow[0:64], facs[0], facs[1]) + o
-            return carry
-
-        lax.fori_loop(0, 12, chunk, 0)
+        sc = nt(qa[...].reshape(NY * TOK, 128), kk[...])
+        probs, facs = [], []
+        for h, (mx, ls) in enumerate(((mx0, ls0), (mx1, ls1))):
+            cols = [sc[:, 128 * (3 * h + j) : 128 * (3 * h + j + 1)] for j in range(3)]
+            old = mx[...]
+            top = jnp.max(jnp.maximum(jnp.maximum(cols[0], cols[1]), cols[2]), axis=1, keepdims=True)
+            new = jnp.maximum(old, top)
+            fac = jnp.exp(old - new)
+            ps = [jnp.exp(v - new) for v in cols]
+            ls[...] = ls[...] * fac + (ps[0] + ps[1] + ps[2])
+            mx[...] = new
+            probs += ps
+            facs.append(fac)
+        pb = jnp.concatenate([p.astype(BF16) for p in probs], axis=1)
+        o = jnp.dot(pb, vv[...], preferred_element_type=F32)
+        acc[...] = acc[...] * jnp.where(qlow, facs[0], facs[1]) + o
 
     for s in range(8):
         got(kv.at[2 * s + 1], kvs.at[0, s], kvr.at[0, s])
@@ -201,10 +192,14 @@
             got(kv.at[2 * s + 2], kvs.at[1, s], kvr.at[1, s])
             if s < 6:
                 kv_ccw(s + 1)
+        if s == 0:
+            for d in range(1, NY):
+                got(qa.at[up(y, -d, NY)], qs.at[d - 1], qr.at[d - 1])
         if s == 1:
             w_start()
-        if s >= 3:
-            pump(s - 3)
+        if s >= 2:
+            pump(2 * s - 4)
+            pump(2 * s - 3)
         if s == 3:
             for e in range(1, NX):
                 got(rs_.at[c, y, up(x, -e, NX)], r1s.at[e - 1], r1r.at[e - 1])
@@ -235,7 +230,8 @@
         dev = (z, yb, x, c)
         go(ssend.at[d - 1], srecv.at[d - 1], ss_.at[d - 1], sr_.at[d - 1], dev)
         go(osend.at[d - 1], orecv.at[d - 1], os_.at[d - 1], or_.at[d - 1], dev)
-    pump(5)
+    pump(12)
+    pump(13)
     mine, st = part_of(y)
     outs, stats = [mine], [st]
     for d in range(1, NY):
@@ -272,25 +268,25 @@
         yb = up(y, -d, NY)
         got(rs_.at[c, yb], r2s.at[d - 1], r2r.at[d - 1])
         go(rs_.at[c, yb], rs_.at[c, yb], rds.at[d], rdr.at[d], partner)
-    for t in range(6, 10):
-        pump(t)
-    for d in range(NY):
+    pump(14)
+    pump(15)
+
+    def forward(d):
         for e in range(NX):
             o = d * NX + e
             if o:
                 sl = aa.at[up(y, -d, NY), :, lanes(up(x, -e, NX) * 2 + c)]
                 got(sl, as_.at[o], ar_.at[o])
                 go(sl, sl, ads.at[o], adr.at[o], partner)
-    for t in range(10, 16):
-        pump(t)
-    for e in range(NX):
-        wr = pl.ds(pl.multiple_of((up(x, -e, NX) * 2 + 1 - c) * 128, 128), 128)
-        got(wo.at[wr], wds.at[e], wdr.at[e])
 
     gain = ng_ref[...]
 
-    def block(d):
+    def project(d):
         yb = up(y, -d, NY)
+        if d == 0:
+            for e in range(NX):
+                wr = pl.ds(pl.multiple_of((up(x, -e, NX) * 2 + 1 - c) * 128, 128), 128)
+                got(wo.at[wr], wds.at[e], wdr.at[e])
         for e in range(NX):
             sl = aa.at[yb, :, lanes(up(x, -e, NX) * 2 + 1 - c)]
             got(sl, ads.at[d * NX + e], adr.at[d * NX + e])
@@ -304,11 +300,30 @@
             mid[r] = v
             sq = jnp.mean(v * v, axis=1, keepdims=True)
             dn[r] = v * lax.rsqrt(sq + EPS) * gain
-        nb[...] = dn[...].astype(BF16)
+        nb[d] = dn[...].astype(BF16)
         if d == 0:
             mown[...] = mid[pl.ds(pl.multiple_of(tp * ROWS, 8), ROWS)]
-        g = nt(nb[...], wm[0:UNITS])
-        u = nt(nb[...], wm[UNITS : 2 * UNITS])
+
+    forward(0)
+    pump(16)
+    forward(1)
+    pump(17)
+    project(0)
+    forward(3)
+    pump(18)
+    project(1)
+    forward(2)
+    pump(19)
+    pump(20)
+    project(3)
+    pump(21)
+    project(2)
+    pump(22)
+    pump(23)
+
+    def block(d):
+        g = nt(nb[d], wm[0:UNITS])
+        u = nt(nb[d], wm[UNITS : 2 * UNITS])
         hid = (g / (1.0 + jnp.exp(-g)) * u).astype(BF16)
         for n in range(4):
             cols = slice(512 * n, 512 * n + 512)
@@ -319,27 +334,70 @@
             dsend[d, e] = dn[pl.ds(pl.multiple_of((xb * 2 + 1 - c) * ROWS, 8), ROWS)].astype(BF16)
         go(dsend.at[d], drecv.at[d], dds.at[d], ddr.at[d], partner)
 
-    def finish(d):
+    HALF = DM // 2
+
+    def first(d):
+        yb = up(y, -d, NY)
         got(drecv.at[d], dds.at[d], ddr.at[d])
         for e in range(NX):
-            o = d * NX + e
-            v = pown[o] + drecv[d, e].astype(F32)
-            if o == 0:
-                osum[...] = v
+            v = pown[d * NX + e] + drecv[d, e].astype(F32)
+            if e:
+                asend[d, e - 1] = v[:, :HALF].astype(BF16)
             else:
-                rsend[o] = v.astype(BF16)
-                go(rsend.at[o], rrecv.at[o], fs.at[o], fr.at[o], (z, up(y, -d, NY), up(x, -e, NX), c))
-
-    for d in range(NY):
-        block(d)
+                aown[d] = v[:, :HALF]
+            if d:
+                bsend[d - 1, e] = v[:, HALF:].astype(BF16)
+            else:
+                bown[e] = v[:, HALF:]
         if d:
-            finish(d - 1)
-    finish(NY - 1)
-    total = osum[...]
-    for o in range(1, NX * NY):
-        got(rrecv.at[o], fs.at[o], fr.at[o])
-        total = total + rrecv[o].astype(F32)
-    out_ref[...] = (mown[...] + 0.5 * total).astype(BF16)
+            go(bsend.at[d - 1], brecv.at[d - 1], f2s.at[d - 1], f2r.at[d - 1], (z, yb, x, c))
+        for e in range(1, NX):
+            dev = (z, y, up(x, -e, NX), c)
+            go(asend.at[d, e - 1], arecv.at[d, e - 1], f1s.at[d, e - 1], f1r.at[d, e - 1], dev)
+
+    def second(d):
+        v = aown[d]
+        for e in range(1, NX):
+            got(arecv.at[d, e - 1], f1s.at[d, e - 1], f1r.at[d, e - 1])
+            v = v + arecv[d, e - 1].astype(F32)
+        if d:
+            a2send[d - 1] = v.astype(BF16)
+            go(a2send.at[d - 1], a2recv.at[d - 1], f3s.at[d - 1], f3r.at[d - 1], (z, up(y, -d, NY), x, c))
+        else:
+            outa[...] = v
+
+    block(2)
+    block(1)
+    first(2)
+    block(3)
+    first(1)
+    block(0)
+    first(3)
+    second(2)
+    first(0)
+    second(1)
+    second(3)
+    for d in range(1, NY):
+        got(brecv.at[d - 1], f2s.at[d - 1], f2r.at[d - 1])
+    for e in range(NX):
+        v = bown[e]
+        for d in range(1, NY):
+            v = v + brecv[d - 1, e].astype(F32)
+        if e:
+            b2send[e - 1] = v.astype(BF16)
+            go(b2send.at[e - 1], b2recv.at[e - 1], f4s.at[e - 1], f4r.at[e - 1], (z, y, up(x, -e, NX), c))
+        else:
+            outb = v
+    second(0)
+    va = outa[...]
+    for d in range(1, NY):
+        got(a2recv.at[d - 1], f3s.at[d - 1], f3r.at[d - 1])
+        va = va + a2recv[d - 1].astype(F32)
+    out_ref[:, :HALF] = (mown[:, :HALF] + 0.5 * va).astype(BF16)
+    for e in range(1, NX):
+        got(b2recv.at[e - 1], f4s.at[e - 1], f4r.at[e - 1])
+        outb = outb + b2recv[e - 1].astype(F32)
+    out_ref[:, HALF:] = (mown[:, HALF:] + 0.5 * outb).astype(BF16)
     for cp in pending:
         cp.wait_send()
 
@@ -377,15 +435,18 @@
         v((NY, TOK, 1024), BF16),
         v((3, TOK, 128), BF16), v((3, TOK, 128), BF16),
         v((3, 32, TOK), F32), v((3, 32, TOK), F32),
-        v((TOK, DM), F32), v((TOK, DM), BF16), v((TOK, DM), F32),
+        v((TOK, DM), F32), v((NY, TOK, DM), BF16), v((TOK, DM), F32),
         v((16, ROWS, DM), F32),
         v((NY, NX, ROWS, DM), BF16), v((NY, NX, ROWS, DM), BF16),
-        v((16, ROWS, DM), BF16), v((16, ROWS, DM), BF16),
-        v((ROWS, DM), F32), v((ROWS, DM), F32),
-        dma((2, 8)), dma((2, 8)), dma((3,)), dma((3,)), dma((3,)), dma((3,)), dma((2, 2, 8)), dma((2, 2, 8)),
+        v((ROWS, DM), F32),
+        v((4, 3, ROWS, DM // 2), BF16), v((4, 3, ROWS, DM // 2), BF16), v((4, ROWS, DM // 2), F32),
+        v((3, 4, ROWS, DM // 2), BF16), v((3, 4, ROWS, DM // 2), BF16), v((4, ROWS, DM // 2), F32),
+        *[v((3, ROWS, DM // 2), BF16)] * 4,
+        v((ROWS, DM // 2), F32),
+        dma((2, 8)), dma((2, 8)), dma((3,)), dma((3,)), dma((3,)), dma((3,)), dma((2, 3, 8)), dma((2, 3, 8)),
         dma((3,)), dma((3,)), dma((3,)), dma((3,)), dma((4,)), dma((4,)), dma((3,)), dma((3,)), dma((4,)), dma((4,)),
         dma((3,)), dma((3,)), dma((3,)), dma((3,)), dma((16,)), dma((16,)), dma((16,)), dma((16,)),
-        dma((4,)), dma((4,)), dma((16,)), dma((16,)),
+        dma((4,)), dma((4,)), dma((4, 3)), dma((4, 3)), *[dma((3,))] * 6,
     ]
     return pl.pallas_call(
         kernel,

time: 122 us -> 96.3 us (0.79)
  Pallas kernels: 118 us -> 92 us
    pallas_call x1, Pallas kernels: 118 us -> 92 us  [body(): pl.pallas_call(kernel, out_shape=jax.ShapeDtypeStruct((ROWS, DM), BF16),...]
where the time goes in v2:
time: 96.3 us; the launch traced here: 96.1 us
  Pallas kernels  92 us (96%)
  local copies, waits for them, and re-layouts  3.45 us (4%)
    pallas_call x1, Pallas kernels, body(): pl.pallas_call(kernel, out_shape=jax.ShapeDtypeStruct((ROWS, DM), BF16),...  92 us
    unnamed x8, local copies, waits for them, and re-layouts  3.38 us

profile of v2, /device:TPU:1, one launch (start us, length us, event | category | flops | bytes accessed | tf_op | source)
XLA Modules:
  0.0 96.1 jit_solution(12658264174309447081)
XLA Ops:
  0.0 0.1 fusion
  0.2 0.1 fusion.1
  0.3 0.1 fusion.2
  0.5 0.0 copy-start.1
  0.5 0.1 fusion.3
  0.6 0.5 copy-done.1
  1.1 0.0 copy-start.2
  1.1 0.1 broadcast_dynamic-update-slice_fusion.1
  1.2 0.6 copy-done.2
  1.8 0.1 broadcast_dynamic-update-slice_fusion.tab_ref
  1.8 0.0 copy-start
  1.8 0.7 copy-done
  2.5 92.0 %layer.1 = bf16[24,2048]{1,0:T(8,128)(2,1)} custom-call(bf16[192,128]{1,0:T(8,128)(2,1)} %q_ref.1, bf16[64,192]{1,0:T(8,128)(2,1)} %bitcast.5, bf16[64,192]{1,0:T(8,128)(2,1)} %bitcast.6, f32[192,192]{1,0:T(8,128)} %copy-done, bf16[32,704]{1,0:T(8,128)(2,1)} %wg_ref.1, bf16[32,704]{1,0:T(8,128)(2,1)} %wu_ref.1, bf16[32,704]{1,0:T(8,128)(2,1)} %bitcast.4, ...), custom_call_target="tpu_custom_call" | custom-call | tf_op jit(solution)/shard_map/layer/pallas_call | solution.py:451
  94.6 1.5 %copy.18 = bf16[24,2048]{1,0:T(8,128)(2,1)} copy(bf16[24,2048]{1,0:T(8,128)(2,1)} %layer.1) | data formatting | bytes 196608
  (2 shorter events, 0.0 us)
Async XLA Ops:
  0.5 0.7 copy-start.1
  1.1 0.7 copy-start.2
  1.8 0.7 copy-start
